TPU v7x, 32 devices: a whole 2x2x4 slice. The times are simulated.
32 devices in a mesh: sp: 8 (over z, core), tp: 4 (over y, x).
Axes of the slice: x: 2, y: 2, z: 4, core: 2. Of those that a mesh axis runs over, the one named last changes fastest.
Arguments:
- resid: bfloat16 [4096, 2048], P(('sp', 'tp')), may hold values from -6 to 6
- branch_input: bfloat16 [1024, 4096], P('tp', 'sp'), may hold values from -6 to 6
- gate_in: bfloat16 [1024, 4096], P('tp', 'sp'), may hold values from -6 to 6
- conv_taps: bfloat16 [4, 1024], P(None, 'tp'), may hold values from -3 to 3
- rate_weight: bfloat16 [16, 64, 64], P('tp'), may hold values from -0.75 to 0.75
- input_weight: bfloat16 [16, 64, 64], P('tp'), may hold values from -0.75 to 0.75
- decay_base: float32 [1024], P('tp')
- decay_extra: float32 [4096], P('sp'), may hold values from -2 to 0
- out_weight: bfloat16 [1024, 2048], P('tp'), may hold values from -0.1875 to 0.1875
- gain_mix: float32 [2048], replicated, may hold values from 0.1 to 1.9
- gain_pre: float32 [2048], replicated, may hold values from 0.1 to 1.9
- gain_post: float32 [2048], replicated, may hold values from 0.1 to 1.9
- expert_ids: int32 [4096, 2], P(('sp', 'tp')), may hold values from 0 to 7, as said below
- route_weight: float32 [4096, 2], P(('sp', 'tp')), may hold values from 0.2 to 1
- gate_proj: bfloat16 [8, 512, 2048], P('sp', 'tp'), may hold values from -0.125 to 0.125
- up_proj: bfloat16 [8, 512, 2048], P('sp', 'tp'), may hold values from -0.125 to 0.125
- down_proj: bfloat16 [8, 512, 2048], P('sp', 'tp'), may hold values from -0.25 to 0.25
Outputs:
- layer_out: bfloat16 [4096, 2048], P(('sp', 'tp'))
Inputs may be any that keep to these rules, and one draw needn't show every extreme that they name: `expert_ids`: each row names two different experts of one group: both lie in g * 2 .. g * 2 + 1 for some g. In each aligned block of 128 rows (the rows of one device) every expert is named by exactly 32 rows.
All inputs are finite; a program needn't handle non-finite values.
Results may differ from a plain program's by a relative error of at most 0.0065.
Values may be sent and summed in bfloat16 or wider, within the bound.
A program may use at most 128 MiB of HBM per device.

v0:
```python
import math
import jax
import jax.numpy as jnp
from jax import lax
from jax.sharding import PartitionSpec as P

epsilon = 1e-06
gate_power = 8.0


def entering_2(array, axis, combine, identity):
    count, here = (lax.axis_size(axis), lax.axis_index(axis))
    everything = jax.tree.map(lambda part: lax.all_gather(part, axis), array)
    start = jax.tree.map(
        lambda part, zero: jnp.broadcast_to(jnp.asarray(zero, part.dtype), part.shape),
        array,
        identity,
    )

    def hop(k, before):
        reached = k < here
        new = combine(before, jax.tree.map(lambda part: part[k], everything))
        return jax.tree.map(lambda a, b: jnp.where(reached, a, b), new, before)

    return lax.fori_loop(0, count, hop, start)


def passed_along(value, axis, steps):
    count = lax.axis_size(axis)
    first, last = (max(0, -steps), min(count, count - steps))
    return lax.ppermute(value, axis, [(source, source + steps) for source in range(first, last)])


def normalized(values, gain):
    return values * lax.rsqrt(jnp.mean(values * values, axis=-1, keepdims=True) + epsilon) * gain


def combine_pair(earlier, latter):
    return (earlier[0] * latter[0], latter[0] * earlier[1] + latter[1])


def carry_in(block_keep, block_state):
    identity = (jnp.ones(block_keep.shape, jnp.float32), jnp.zeros(block_state.shape, jnp.float32))
    return entering_2((block_keep, block_state), "sp", combine_pair, identity)


def block_cumsum(log_keep):
    channels, positions = log_keep.shape
    span = math.gcd(positions, 128)
    count = positions // span
    shaped = log_keep.reshape(channels, count, span)
    inner = jnp.cumsum(shaped, axis=2)
    before = jnp.cumsum(inner[:, :, -1], axis=1) - inner[:, :, -1]
    return (inner + before[:, :, None]).reshape(channels, positions)


def block_recurrence(log_keep, driven, start_state):
    channels, positions = log_keep.shape
    span = math.gcd(positions, 128)
    count = positions // span
    order = jnp.arange(span, dtype=jnp.int32)
    lower = (order[:, None] >= order[None, :])[None, :, :]

    def one_block(index, carried):
        state, total_log, states_out, logs_out = carried
        first = index * span
        block_log = lax.dynamic_slice_in_dim(log_keep, first, span, 1)
        block_drive = lax.dynamic_slice_in_dim(driven, first, span, 1)
        running = jnp.cumsum(block_log, axis=1)
        gap = jnp.where(lower, running[:, :, None] - running[:, None, :], -jnp.inf)
        inner = jnp.einsum("cts,cs->ct", jnp.exp(gap), block_drive, precision=lax.Precision.HIGHEST)
        produced = inner + jnp.exp(running) * state[:, None]
        whole_log = running + total_log[:, None]
        states_out = lax.dynamic_update_slice_in_dim(states_out, produced, first, 1)
        logs_out = lax.dynamic_update_slice_in_dim(logs_out, whole_log, first, 1)
        return (produced[:, -1], whole_log[:, -1], states_out, logs_out)

    initial = (
        start_state,
        jnp.zeros((channels,), jnp.float32),
        jnp.zeros((channels, positions), jnp.float32),
        jnp.zeros((channels, positions), jnp.float32),
    )
    _, _, hidden_state, summed_log = lax.fori_loop(0, count, one_block, initial)
    return (hidden_state, summed_log)


def per_device(
    resid,
    branch_input,
    gate_in,
    conv_taps,
    rate_weight,
    input_weight,
    decay_base,
    decay_extra,
    out_weight,
    gain_mix,
    gain_pre,
    gain_post,
    expert_ids,
    route_weight,
    gate_proj,
    up_proj,
    down_proj,
):
    channels, positions = branch_input.shape
    tap_count = conv_taps.shape[0]
    edge_cols = passed_along(branch_input[:, positions - (tap_count - 1) :], "sp", 1)
    padded = jnp.concatenate([edge_cols, branch_input], axis=1).astype(jnp.float32)
    filter_tap_weights = conv_taps.astype(jnp.float32)
    convolved = filter_tap_weights[0][:, None] * padded[:, 0:positions]
    for offset in range(1, tap_count):
        convolved = (
            convolved + filter_tap_weights[offset][:, None] * padded[:, offset : offset + positions]
        )
    grouped = convolved.reshape(rate_weight.shape[0], rate_weight.shape[1], positions)
    rate_gate = jax.nn.sigmoid(
        jnp.einsum(
            "ncs,ncd->nds",
            grouped,
            rate_weight.astype(jnp.float32),
            precision=lax.Precision.HIGHEST,
        ).reshape(channels, positions)
    )
    input_gate = jax.nn.sigmoid(
        jnp.einsum(
            "ncs,ncd->nds",
            grouped,
            input_weight.astype(jnp.float32),
            precision=lax.Precision.HIGHEST,
        ).reshape(channels, positions)
    )
    decay_rate = -gate_power * jax.nn.softplus(-decay_base)
    log_keep = decay_rate[:, None] * rate_gate + decay_extra[None, :]
    driven = jnp.sqrt(-jnp.expm1(2.0 * log_keep)) * input_gate * convolved
    summed_log = block_cumsum(log_keep)
    tail_keep = jnp.exp(summed_log[:, -1:] - summed_log)
    _, entering = carry_in(jnp.exp(summed_log[:, -1]), jnp.sum(driven * tail_keep, axis=1))
    hidden_state = block_recurrence(log_keep, driven, entering)[0]
    branch_out = (hidden_state * jax.nn.gelu(gate_in.astype(jnp.float32), approximate=True)).astype(
        jnp.bfloat16
    )
    token_rows = lax.all_to_all(branch_out, "tp", split_axis=1, concat_axis=0, tiled=True)
    token_count = token_rows.shape[1]
    mixed_rows = lax.dot_general(
        token_rows,
        lax.all_gather(out_weight, "tp", axis=0, tiled=True),
        (((0,), (0,)), ((), ())),
        preferred_element_type=jnp.float32,
    )
    after_mix = resid.astype(jnp.float32) + normalized(mixed_rows, gain_mix)
    ffn_in = normalized(after_mix, gain_pre).astype(jnp.bfloat16)
    top_count = expert_ids.shape[1]
    experts = gate_proj.shape[0] * lax.axis_size("sp")
    capacity = top_count * token_count // experts
    chosen = expert_ids.reshape(-1)
    matches = (chosen[:, None] == jnp.arange(experts, dtype=jnp.int32)[None, :]).astype(jnp.int32)
    slot_index = jnp.sum((jnp.cumsum(matches, axis=0) - 1) * matches, axis=1)
    target = chosen * capacity + slot_index
    source = (
        jnp.zeros((experts * capacity,), jnp.int32)
        .at[target]
        .set(jnp.arange(token_count * top_count, dtype=jnp.int32) // top_count)
    )
    outgoing = ffn_in[source].reshape(experts, capacity, ffn_in.shape[1])
    arriving = lax.all_to_all(outgoing, "sp", split_axis=0, concat_axis=1, tiled=True)
    gate_rows = lax.all_gather(gate_proj, "tp", axis=1, tiled=True)
    up_rows = lax.all_gather(up_proj, "tp", axis=1, tiled=True)
    down_rows = lax.all_gather(down_proj, "tp", axis=1, tiled=True)
    gate_vals = jnp.einsum("emd,ekd->emk", arriving, gate_rows, preferred_element_type=jnp.float32)
    up_vals = jnp.einsum("emd,ekd->emk", arriving, up_rows, preferred_element_type=jnp.float32)
    hidden = (jax.nn.silu(gate_vals) * up_vals).astype(jnp.bfloat16)
    result = jnp.einsum("emk,ekd->emd", hidden, down_rows, preferred_element_type=jnp.float32)
    returned = lax.all_to_all(
        result.astype(jnp.bfloat16), "sp", split_axis=1, concat_axis=0, tiled=True
    )
    returned = returned.reshape(experts * capacity, returned.shape[2])
    picked = returned[target].astype(jnp.float32).reshape(token_count, top_count, returned.shape[1])
    moe = jnp.sum(picked * route_weight[:, :, None], axis=1)
    return (after_mix + normalized(moe, gain_post)).astype(jnp.bfloat16)


def solution(mesh):
    in_specs = (
        P(("sp", "tp"), None),
        P("tp", "sp"),
        P("tp", "sp"),
        P(None, "tp"),
        P("tp", None, None),
        P("tp", None, None),
        P("tp"),
        P("sp"),
        P("tp", None),
        P(),
        P(),
        P(),
        P(("sp", "tp"), None),
        P(("sp", "tp"), None),
        P("sp", "tp", None),
        P("sp", "tp", None),
        P("sp", "tp", None),
    )
    out_specs = P(("sp", "tp"), None)
    return jax.shard_map(
        per_device, mesh=mesh, in_specs=in_specs, out_specs=out_specs, check_vma=False
    )
```

profile of v0, /device:TPU:0, one launch (start us, length us, event | category | flops | bytes accessed | tf_op | source)
XLA Modules:
  0.0 288.3 jit_solution(16945330147929977153)
XLA Ops:
  6.6 0.7 all-gather.8.cloned.1.call-update
  7.3 0.7 all-gather.10.cloned.1.call-update
  8.1 0.7 all-gather.12.cloned.1.call-update
  8.9 2.4 collective-permute-start
  11.8 0.6 reduce-window.6
  12.4 0.2 slice_reduce_fusion
  13.2 1.4 scatter_custom_fusion
  14.8 0.6 fusion.39
  15.4 0.5 fusion.24
  16.1 0.3 copy.81
  16.4 0.2 fusion.49
  16.8 0.2 copy.85
  17.2 0.5 fusion.26
  17.7 0.9 multiply_reduce_fusion.4
  18.6 13.4 %all-gather.2 = f32[8,1,256]{2,1,0:T(1,128)S(1)} all-gather(f32[1,1,256]{2,1,0:T(1,128)S(1)} %bitcast.139), channel_id=3, replica_groups=mesh['sp'=8,'tp'=4] {'sp'}, dimensions={0}, use_global_device_ids=true | all-gather | bytes 9216 | tf_op jit(solution)/shard_map/all_gather | solution.py:13
  32.0 8.7 %all-gather = f32[2048,1]{0,1:T(1,128)S(1)} all-gather(f32[256,1]{0,1:T(1,128)S(1)} %get-tuple-element.288), channel_id=2, replica_groups=mesh['sp'=8,'tp'=4] {'sp'}, dimensions={0}, use_global_device_ids=true | all-gather | bytes 9216 | tf_op jit(solution)/shard_map/all_gather | solution.py:13
  40.7 0.6 broadcast.207
  41.3 0.7 reduce.5
  42.0 0.4 while.31
  42.5 126.3 %while.30 = (s32[]{:T(128)}, f32[256]{0:T(256)S(1)}, f32[256,512]{1,0:T(8,128)S(1)}, f32[256,512]{1,0:T(8,128)S(1)}, f32[256,512]{1,0:T(8,128)S(1)}, /*index=5*/...) while((s32[]{:T(128)}, f32[256]{0:T(256)S(1)}, f32[256,512]{1,0:T(8,128)S(1)}, ...), condition=%wide.region_7.8_spmd.clone, body=%wide.region_5.7_spmd.clone.sunk | while | flops 62963716 | bytes 2919583 | solution.py:84
  57.0 27.2 %fusion.83 = f32[256,1,128]{2,1,0:T(1,128)S(1)} fusion(f32[256,128,1]{1,2,0:T(1,128)S(1)} %bitcast.110, f32[256,128]{1,0:T(8,128)S(1)} %copy.123, pred[128,128]{1,0:T(8,128)(4,1)S(1)} %fusion.82), kind=kOutput, calls=%fused_computation.4.clone.1 | convolution fusion | flops 58720256 | bytes 409600 | tf_op jit(solution)/shard_map/while/body/eval_jaxpr/cts,cs->ct/dot_general | solution.py:71
  85.0 27.2 %fusion.83 = f32[256,1,128]{2,1,0:T(1,128)S(1)} fusion(f32[256,128,1]{1,2,0:T(1,128)S(1)} %bitcast.110, f32[256,128]{1,0:T(8,128)S(1)} %copy.123, pred[128,128]{1,0:T(8,128)(4,1)S(1)} %fusion.82), kind=kOutput, calls=%fused_computation.4.clone.1 | convolution fusion | flops 58720256 | bytes 409600 | tf_op jit(solution)/shard_map/while/body/eval_jaxpr/cts,cs->ct/dot_general | solution.py:71
  112.7 0.2 reduce_window_sum.57
  113.0 27.2 %fusion.83 = f32[256,1,128]{2,1,0:T(1,128)S(1)} fusion(f32[256,128,1]{1,2,0:T(1,128)S(1)} %bitcast.110, f32[256,128]{1,0:T(8,128)S(1)} %copy.123, pred[128,128]{1,0:T(8,128)(4,1)S(1)} %fusion.82), kind=kOutput, calls=%fused_computation.4.clone.1 | convolution fusion | flops 58720256 | bytes 409600 | tf_op jit(solution)/shard_map/while/body/eval_jaxpr/cts,cs->ct/dot_general | solution.py:71
  141.0 27.2 %fusion.83 = f32[256,1,128]{2,1,0:T(1,128)S(1)} fusion(f32[256,128,1]{1,2,0:T(1,128)S(1)} %bitcast.110, f32[256,128]{1,0:T(8,128)S(1)} %copy.123, pred[128,128]{1,0:T(8,128)(4,1)S(1)} %fusion.82), kind=kOutput, calls=%fused_computation.4.clone.1 | convolution fusion | flops 58720256 | bytes 409600 | tf_op jit(solution)/shard_map/while/body/eval_jaxpr/cts,cs->ct/dot_general | solution.py:71
  168.8 0.9 copy_bitcast_fusion.1
  169.7 3.7 %all-to-all-start = ((bf16[256,4,128]{2,0,1:T(8,128)(2,1)}), bf16[256,4,128]{2,0,1:T(8,128)(2,1)S(1)}, u32[]{:S(2)}, u32[]{:S(2)}) async-start(bf16[256,4,128]{2,0,1:T(8,128)(2,1)} %copy_bitcast_fusion.1), calls=%async_computation | async-start | bytes 524288 | tf_op jit(solution)/shard_map/all_to_all | solution.py:144
  173.4 5.9 %all-to-all-done = bf16[256,4,128]{2,0,1:T(8,128)(2,1)S(1)} async-done(((bf16[256,4,128]{2,0,1:T(8,128)(2,1)}), bf16[256,4,128]{2,0,1:T(8,128)(2,1)S(1)}, u32[]{:S(2)}, u32[]{:S(2)}) %all-to-all-start) | async-done | bytes 262176 | tf_op jit(solution)/shard_map/all_to_all | solution.py:144
  179.3 3.1 %multiply_reduce_fusion.3 = (f32[128]{0:T(128)S(1)}, f32[128,2048]{1,0:T(8,128)S(1)}) fusion(bf16[1024,128]{1,0:T(8,128)(2,1)S(1)} %bitcast.116, bf16[1024,2048]{1,0:T(8,128)(2,1)} %all-gather.8.cloned.1.call-done), kind=kOutput, calls=%fused_computation.46 | convolution fusion | flops 537395072 | bytes 5505536 | tf_op jit(solution)/shard_map/dot_general | solution.py:146
  182.4 0.4 multiply_reduce_fusion.2
  182.8 0.3 multiply_convert_fusion
  183.1 2.3 gather_fusion
  185.4 3.6 %all-to-all-start.1 = ((bf16[8,32,2048]{2,1,0:T(8,128)(2,1)}), bf16[8,32,2048]{2,1,0:T(8,128)(2,1)S(1)}, u32[]{:S(2)}, u32[]{:S(2)}) async-start(bf16[8,32,2048]{2,1,0:T(8,128)(2,1)} %bitcast.20), calls=%async_computation.1 | async-start | bytes 2097152 | tf_op jit(solution)/shard_map/all_to_all | solution.py:167
  189.0 26.5 %all-to-all-done.1 = bf16[8,32,2048]{2,1,0:T(8,128)(2,1)S(1)} async-done(((bf16[8,32,2048]{2,1,0:T(8,128)(2,1)}), bf16[8,32,2048]{2,1,0:T(8,128)(2,1)S(1)}, u32[]{:S(2)}, u32[]{:S(2)}) %all-to-all-start.1) | async-done | bytes 1048608 | tf_op jit(solution)/shard_map/all_to_all | solution.py:167
  215.5 2.3 fusion.16
  217.9 4.6 %fusion.12 = bf16[1,256,2048]{2,1,0:T(8,128)(2,1)} fusion(bf16[1,512,2048]{2,1,0:T(8,128)(2,1)} %all-gather.14.cloned.1.call-done, bf16[256,2048]{1,0:T(8,128)(2,1)S(1)} %bitcast.118, bf16[1,512,2048]{2,1,0:T(8,128)(2,1)} %all-gather.12.cloned.1.call-done, f32[256,512]{1,0:T(8,128)S(1)} %fusion.16), kind=kOutput, calls=%fused_computation.23 | convolution fusion | flops 1075052544 | bytes 6815744 | tf_op jit(solution)/shard_map/emk,ekd->emd/dot_general | solution.py:174
  222.5 2.8 copy.117
  225.3 0.5 broadcast.210
  225.8 7.8 %reduce.6 = bf16[256,2048]{1,0:T(8,128)(2,1)} reduce(bf16[256,1,2048]{2,1,0:T(2,128)(2,1)S(1)} %bitcast.109, bf16[]{:T(256)} %broadcast.210), dimensions={1}, to_apply=%bitcast.89.reduce_sub_computation | reduce | bytes 2097154
  233.6 2.6 reshape.255
  236.3 3.8 %all-to-all-start.2 = ((bf16[8,2,32768]{2,1,0:T(2,128)(2,1)}), bf16[8,2,32768]{2,1,0:T(2,128)(2,1)S(1)}, u32[]{:S(2)}, u32[]{:S(2)}) async-start(bf16[8,2,32768]{2,1,0:T(2,128)(2,1)} %reshape.255), calls=%async_computation.2 | async-start | bytes 2097152 | tf_op jit(solution)/shard_map/all_to_all | solution.py:175
  240.2 26.3 %all-to-all-done.2 = bf16[8,2,32768]{2,1,0:T(2,128)(2,1)S(1)} async-done(((bf16[8,2,32768]{2,1,0:T(2,128)(2,1)}), bf16[8,2,32768]{2,1,0:T(2,128)(2,1)S(1)}, u32[]{:S(2)}, u32[]{:S(2)}) %all-to-all-start.2) | async-done | bytes 1048608 | tf_op jit(solution)/shard_map/all_to_all | solution.py:175
  266.5 3.5 %reshape.256 = bf16[256,1,2048]{2,1,0:T(2,128)(2,1)} reshape(bf16[8,2,32768]{2,1,0:T(2,128)(2,1)S(1)} %all-to-all-done.2) | data formatting | bytes 2097152
  270.0 2.2 copy.115
  272.2 2.3 gather_fusion.1
  274.5 2.4 reshape.210
  276.9 3.2 %multiply_reduce_fusion = f32[128,2048]{1,0:T(8,128)S(1)} fusion(f32[128,2,2048]{2,1,0:T(2,128)S(1)} %reshape.210, f32[128,2]{1,0:T(8,128)S(1)} %copy.93), kind=kLoop, calls=%fused_computation.29 | loop fusion | flops 786432 | bytes 3146752 | tf_op jit(solution)/shard_map/reduce_sum | solution.py:180
  280.3 1.2 add_convert_fusion
  (130 shorter events, 5.1 us)
Async XLA Ops:
  6.5 8.9 %copy-start = (bf16[4,64,64]{2,1,0:T(8,128)(2,1)S(1)}, bf16[4,64,64]{2,1,0:T(8,128)(2,1)}, u32[]{:S(2)}) copy-start(bf16[4,64,64]{2,1,0:T(8,128)(2,1)} %param.25) | copy-start | bytes 98308
  6.5 2.3 copy-start.3
  6.5 4.8 %copy-start.10 = (s32[128,2]{0,1:T(2,128)S(1)}, s32[128,2]{0,1:T(2,128)}, u32[]{:S(2)}) copy-start(s32[128,2]{0,1:T(2,128)} %param.33) | copy-start | bytes 3076
  6.5 5.2 %copy-start.9 = (bf16[4,256]{1,0:T(4,128)(2,1)S(1)}, bf16[4,256]{1,0:T(4,128)(2,1)}, u32[]{:S(2)}) copy-start(bf16[4,256]{1,0:T(4,128)(2,1)} %param.24) | copy-start | bytes 6148
  6.5 5.3 %copy-start.12 = (f32[256]{0:T(256)S(1)}, f32[256]{0:T(256)}, u32[]{:S(2)}) copy-start(f32[256]{0:T(256)} %param.27) | copy-start | bytes 3076
  6.5 6.5 %copy-start.8 = (f32[512]{0:T(512)S(1)}, f32[512]{0:T(512)}, u32[]{:S(2)}) copy-start(f32[512]{0:T(512)} %param.28) | copy-start | bytes 6148
  6.6 172.7 %all-gather.8.cloned.1.call-start = ((), (), s32[]{:S(2)}) async-start(), calls=%async_computation.3 | async-start | bytes 5242880 | tf_op jit(solution)/shard_map/all_gather | solution.py:148
  7.3 181.7 %all-gather.10.cloned.1.call-start = ((), (), s32[]{:S(2)}) async-start(), calls=%async_computation.4 | async-start | bytes 2621440 | tf_op jit(solution)/shard_map/all_gather | solution.py:168
  8.0 209.8 %all-gather.12.cloned.1.call-start = ((), (), s32[]{:S(2)}) async-start(), calls=%async_computation.5 | async-start | bytes 2621440 | tf_op jit(solution)/shard_map/all_gather | solution.py:169
  8.8 209.1 %all-gather.14.cloned.1.call-start = ((), (), s32[]{:S(2)}) async-start(), calls=%async_computation.6 | async-start | bytes 2621440 | tf_op jit(solution)/shard_map/all_gather | solution.py:170
  8.9 5.7 %collective-permute-start = (bf16[256,3]{1,0:T(8,128)(2,1)S(1)}, bf16[256,3]{1,0:T(8,128)(2,1)S(1)}, u32[]{:S(2)}, u32[]{:S(2)}) collective-permute-start(bf16[256,3]{1,0:T(8,128)(2,1)S(1)} %slice.49), channel_id=1, source_target_pairs={{0,4},{4,8},{8,12},{12,16},{16,20},{20,24},{24,28},{1,5},{5,9},{9,... | collective-permute-start | bytes 4616 | tf_op jit(solution)/shard_map/ppermute | solution.py:31
  16.3 0.8 copy-start.13
  42.5 126.3 %copy-start.4 = (bf16[256,512]{1,0:T(8,128)(2,1)S(1)}, bf16[256,512]{1,0:T(8,128)(2,1)}, u32[]{:S(2)}) copy-start(bf16[256,512]{1,0:T(8,128)(2,1)} %param.23) | copy-start | bytes 786436
  169.7 9.6 %all-to-all-start = ((bf16[256,4,128]{2,0,1:T(8,128)(2,1)}), bf16[256,4,128]{2,0,1:T(8,128)(2,1)S(1)}, u32[]{:S(2)}, u32[]{:S(2)}) async-start(bf16[256,4,128]{2,0,1:T(8,128)(2,1)} %copy_bitcast_fusion.1), calls=%async_computation | async-start | bytes 524288 | tf_op jit(solution)/shard_map/all_to_all | solution.py:144
  179.3 3.1 %copy-start.1 = (bf16[128,2048]{1,0:T(8,128)(2,1)S(1)}, bf16[128,2048]{1,0:T(8,128)(2,1)}, u32[]{:S(2)}) copy-start(bf16[128,2048]{1,0:T(8,128)(2,1)} %param.21) | copy-start | bytes 1572868
  179.3 3.1 %copy-start.5 = (f32[2048]{0:T(1024)S(1)}, f32[2048]{0:T(1024)}, u32[]{:S(2)}) copy-start(f32[2048]{0:T(1024)} %param.30) | copy-start | bytes 24580
  179.3 3.5 %copy-start.6 = (f32[2048]{0:T(1024)S(1)}, f32[2048]{0:T(1024)}, u32[]{:S(2)}) copy-start(f32[2048]{0:T(1024)} %param.31) | copy-start | bytes 24580
  185.4 30.1 %all-to-all-start.1 = ((bf16[8,32,2048]{2,1,0:T(8,128)(2,1)}), bf16[8,32,2048]{2,1,0:T(8,128)(2,1)S(1)}, u32[]{:S(2)}, u32[]{:S(2)}) async-start(bf16[8,32,2048]{2,1,0:T(8,128)(2,1)} %bitcast.20), calls=%async_computation.1 | async-start | bytes 2097152 | tf_op jit(solution)/shard_map/all_to_all | solution.py:167
  233.6 6.4 %copy-start.11 = (f32[128,2]{0,1:T(2,128)S(1)}, f32[128,2]{0,1:T(2,128)}, u32[]{:S(2)}) copy-start(f32[128,2]{0,1:T(2,128)} %param.34) | copy-start | bytes 3076
  236.3 30.3 %all-to-all-start.2 = ((bf16[8,2,32768]{2,1,0:T(2,128)(2,1)}), bf16[8,2,32768]{2,1,0:T(2,128)(2,1)S(1)}, u32[]{:S(2)}, u32[]{:S(2)}) async-start(bf16[8,2,32768]{2,1,0:T(2,128)(2,1)} %reshape.255), calls=%async_computation.2 | async-start | bytes 2097152 | tf_op jit(solution)/shard_map/all_to_all | solution.py:175
  276.9 3.4 %copy-start.2 = (bf16[128,2048]{1,0:T(8,128)(2,1)S(1)}, bf16[128,2048]{1,0:T(8,128)(2,1)}, u32[]{:S(2)}) copy-start(bf16[128,2048]{1,0:T(8,128)(2,1)} %param.21) | copy-start | bytes 1572868
  276.9 3.4 %copy-start.7 = (f32[2048]{0:T(1024)S(1)}, f32[2048]{0:T(1024)}, u32[]{:S(2)}) copy-start(f32[2048]{0:T(1024)} %param.32) | copy-start | bytes 24580
Sparse Core Ops, SparseCore 0:
  9.2 55.2 all-gather.7
  66.4 35.1 all-gather.9
  103.4 35.1 all-gather.11
  140.4 35.1 all-gather.13
where the time goes:
time: 293 us; the launch traced here: 288 us
  matrix products  120 us (41%)
  waiting for transfers between devices  60.8 us (21%)
  local copies, waits for them, and re-layouts  24.8 us (8%)
  blocking collectives  22.1 us (8%)
  other arithmetic  18.4 us (6%)
  loops' own time  14.9 us (5%)
  between operations  13.8 us (5%)
  starting transfers between devices  13.6 us (5%)
    dot_general x4, matrix products, one_block(): jnp.einsum('cts,cs->ct', jnp.exp(gap), block_drive, precision=lax.Precisi...  109 us
    all_to_all x1, waiting for transfers between devices, per_device(): lax.all_to_all(outgoing, 'sp', split_axis=0, concat_axis=1, tiled=True)  26.5 us
    all_to_all x1, waiting for transfers between devices, per_device(): lax.all_to_all(result.astype(jnp.bfloat16), 'sp', split_axis=1, concat_ax...  26.3 us
    all_gather x2, blocking collectives, entering_2(): everything = jax.tree.map(lambda part: lax.all_gather(part, axis), array)  22.1 us
    another operation x1, loops' own time, block_recurrence(): _, _, hidden_state, summed_log = lax.fori_loop(0, count, one_block, initial)  14.7 us
    unnamed x36, local copies, waits for them, and re-layouts  9.28 us
    unnamed x2, other arithmetic  7.79 us
  transfers between devices with their start and end apart: 8, of which 3 were waited for; matrix products, arithmetic and copies ran while one was open for 45% of the time, Pallas kernels for 0%

commit v1 on v0

--- a/solution.py
+++ b/solution.py
@@ -3,6 +3,7 @@
 import jax.numpy as jnp
 from jax import lax
 from jax.sharding import PartitionSpec as P
+from jax.lax import all_to_all, axis_size
 
 epsilon = 1e-06
 gate_power = 8.0
@@ -104,6 +105,12 @@
     up_proj,
     down_proj,
 ):
+
+    def drive_the_racks(arr, dev_axis):
+        ready = jnp.stack(jnp.split(arr, axis_size(dev_axis), axis=1), axis=0)
+        f_next = all_to_all(ready, dev_axis, 0, 0)
+        return jnp.concatenate(f_next, axis=0)
+
     channels, positions = branch_input.shape
     tap_count = conv_taps.shape[0]
     edge_cols = passed_along(branch_input[:, positions - (tap_count - 1) :], "sp", 1)
@@ -172,9 +179,7 @@
     up_vals = jnp.einsum("emd,ekd->emk", arriving, up_rows, preferred_element_type=jnp.float32)
     hidden = (jax.nn.silu(gate_vals) * up_vals).astype(jnp.bfloat16)
     result = jnp.einsum("emk,ekd->emd", hidden, down_rows, preferred_element_type=jnp.float32)
-    returned = lax.all_to_all(
-        result.astype(jnp.bfloat16), "sp", split_axis=1, concat_axis=0, tiled=True
-    )
+    returned = drive_the_racks(result.astype(jnp.bfloat16), dev_axis="sp")
     returned = returned.reshape(experts * capacity, returned.shape[2])
     picked = returned[target].astype(jnp.float32).reshape(token_count, top_count, returned.shape[1])
     moe = jnp.sum(picked * route_weight[:, :, None], axis=1)

time: 293 us -> 279 us (0.952)
  other arithmetic: 18.4 us -> 10.7 us
  local copies, waits for them, and re-layouts: 24.8 us -> 18.4 us
    unnamed x2 -> x1, other arithmetic: 7.79 us -> 0.01 us
    unnamed x36 -> x39, local copies, waits for them, and re-layouts: 9.28 us -> 5.11 us
  transfers between devices with their start and end apart: 8 -> 8, of which waited for: 3 -> 3; matrix products, arithmetic and copies ran while one was open for 45% -> 48% of each run, Pallas kernels for 0% -> 0%
where the time goes in v1:
time: 279 us; the launch traced here: 274 us
  matrix products  120 us (43%)
  waiting for transfers between devices  60.8 us (22%)
  blocking collectives  22.1 us (8%)
  local copies, waits for them, and re-layouts  18.4 us (7%)
  loops' own time  14.8 us (5%)
  between operations  13.9 us (5%)
  starting transfers between devices  13.4 us (5%)
  other arithmetic  10.7 us (4%)
    dot_general x4, matrix products, one_block(): jnp.einsum('cts,cs->ct', jnp.exp(gap), block_drive, precision=lax.Precisi...  109 us
    all_to_all x1, waiting for transfers between devices, per_device(): lax.all_to_all(outgoing, 'sp', split_axis=0, concat_axis=1, tiled=True)  26.5 us
    all_to_all x1, waiting for transfers between devices, drive_the_racks(): f_next = all_to_all(ready, dev_axis, 0, 0)  26.4 us
    all_gather x2, blocking collectives, entering_2(): everything = jax.tree.map(lambda part: lax.all_gather(part, axis), array)  22.1 us
    another operation x1, loops' own time, block_recurrence(): _, _, hidden_state, summed_log = lax.fori_loop(0, count, one_block, initial)  14.6 us
    all_to_all x1, waiting for transfers between devices, per_device(): lax.all_to_all(branch_out, 'tp', split_axis=1, concat_axis=0, tiled=True)  5.86 us
  transfers between devices with their start and end apart: 8, of which 3 were waited for; matrix products, arithmetic and copies ran while one was open for 48% of the time, Pallas kernels for 0%

profile of v1, /device:TPU:0, one launch (start us, length us, event | category | flops | bytes accessed | tf_op | source)
XLA Modules:
  0.0 274.0 jit_solution(13760332130114189561)
XLA Ops:
  6.6 0.7 all-gather.8.cloned.1.call-update
  7.3 0.7 all-gather.10.cloned.1.call-update
  8.1 0.7 all-gather.12.cloned.1.call-update
  8.9 2.4 collective-permute-start
  11.8 0.6 reduce-window.6
  12.4 0.2 slice_reduce_fusion
  13.2 1.4 scatter_custom_fusion
  14.8 0.6 fusion.39
  15.4 0.5 fusion.24
  16.1 0.3 copy.65
  16.4 0.2 fusion.49
  17.2 0.5 fusion.26
  17.7 0.9 multiply_reduce_fusion.4
  18.6 13.4 %all-gather.2 = f32[8,1,256]{2,1,0:T(1,128)S(1)} all-gather(f32[1,1,256]{2,1,0:T(1,128)S(1)} %bitcast.163), channel_id=3, replica_groups=mesh['sp'=8,'tp'=4] {'sp'}, dimensions={0}, use_global_device_ids=true | all-gather | bytes 9216 | tf_op jit(solution)/shard_map/all_gather | solution.py:14
  32.0 8.7 %all-gather = f32[2048,1]{0,1:T(1,128)S(1)} all-gather(f32[256,1]{0,1:T(1,128)S(1)} %get-tuple-element.283), channel_id=2, replica_groups=mesh['sp'=8,'tp'=4] {'sp'}, dimensions={0}, use_global_device_ids=true | all-gather | bytes 9216 | tf_op jit(solution)/shard_map/all_gather | solution.py:14
  40.8 0.5 broadcast.207
  41.3 0.6 reduce.5
  41.9 0.4 while.31
  42.5 126.2 %while.30 = (s32[]{:T(128)}, f32[256]{0:T(256)S(1)}, f32[256,512]{1,0:T(8,128)S(1)}, f32[256,512]{1,0:T(8,128)S(1)}, f32[256,512]{1,0:T(8,128)S(1)}, /*index=5*/...) while((s32[]{:T(128)}, f32[256]{0:T(256)S(1)}, f32[256,512]{1,0:T(8,128)S(1)}, ...), condition=%wide.region_7.8_spmd.clone, body=%wide.region_5.7_spmd.clone.sunk | while | flops 62963716 | bytes 2919583 | solution.py:85
  56.9 27.2 %fusion.91 = f32[256,1,128]{2,1,0:T(1,128)S(1)} fusion(f32[256,128,1]{1,2,0:T(1,128)S(1)} %bitcast.134, f32[256,128]{1,0:T(8,128)S(1)} %copy.101, pred[128,128]{1,0:T(8,128)(4,1)S(1)} %fusion.90), kind=kOutput, calls=%fused_computation.4.clone.1 | convolution fusion | flops 58720256 | bytes 409600 | tf_op jit(solution)/shard_map/while/body/eval_jaxpr/cts,cs->ct/dot_general | solution.py:72
  84.9 27.2 %fusion.91 = f32[256,1,128]{2,1,0:T(1,128)S(1)} fusion(f32[256,128,1]{1,2,0:T(1,128)S(1)} %bitcast.134, f32[256,128]{1,0:T(8,128)S(1)} %copy.101, pred[128,128]{1,0:T(8,128)(4,1)S(1)} %fusion.90), kind=kOutput, calls=%fused_computation.4.clone.1 | convolution fusion | flops 58720256 | bytes 409600 | tf_op jit(solution)/shard_map/while/body/eval_jaxpr/cts,cs->ct/dot_general | solution.py:72
  112.9 27.2 %fusion.91 = f32[256,1,128]{2,1,0:T(1,128)S(1)} fusion(f32[256,128,1]{1,2,0:T(1,128)S(1)} %bitcast.134, f32[256,128]{1,0:T(8,128)S(1)} %copy.101, pred[128,128]{1,0:T(8,128)(4,1)S(1)} %fusion.90), kind=kOutput, calls=%fused_computation.4.clone.1 | convolution fusion | flops 58720256 | bytes 409600 | tf_op jit(solution)/shard_map/while/body/eval_jaxpr/cts,cs->ct/dot_general | solution.py:72
  140.9 27.2 %fusion.91 = f32[256,1,128]{2,1,0:T(1,128)S(1)} fusion(f32[256,128,1]{1,2,0:T(1,128)S(1)} %bitcast.134, f32[256,128]{1,0:T(8,128)S(1)} %copy.101, pred[128,128]{1,0:T(8,128)(4,1)S(1)} %fusion.90), kind=kOutput, calls=%fused_computation.4.clone.1 | convolution fusion | flops 58720256 | bytes 409600 | tf_op jit(solution)/shard_map/while/body/eval_jaxpr/cts,cs->ct/dot_general | solution.py:72
  168.6 0.9 copy_bitcast_fusion
  169.5 3.7 %all-to-all-start = ((bf16[256,4,128]{2,0,1:T(8,128)(2,1)}), bf16[256,4,128]{2,0,1:T(8,128)(2,1)S(1)}, u32[]{:S(2)}, u32[]{:S(2)}) async-start(bf16[256,4,128]{2,0,1:T(8,128)(2,1)} %copy_bitcast_fusion), calls=%async_computation | async-start | bytes 524288 | tf_op jit(solution)/shard_map/all_to_all | solution.py:151
  173.3 5.9 %all-to-all-done = bf16[256,4,128]{2,0,1:T(8,128)(2,1)S(1)} async-done(((bf16[256,4,128]{2,0,1:T(8,128)(2,1)}), bf16[256,4,128]{2,0,1:T(8,128)(2,1)S(1)}, u32[]{:S(2)}, u32[]{:S(2)}) %all-to-all-start) | async-done | bytes 262176 | tf_op jit(solution)/shard_map/all_to_all | solution.py:151
  179.1 3.1 %multiply_reduce_fusion.3 = (f32[128]{0:T(128)S(1)}, f32[128,2048]{1,0:T(8,128)S(1)}) fusion(bf16[1024,128]{1,0:T(8,128)(2,1)S(1)} %bitcast.140, bf16[1024,2048]{1,0:T(8,128)(2,1)} %all-gather.8.cloned.1.call-done), kind=kOutput, calls=%fused_computation.45 | convolution fusion | flops 537395072 | bytes 5505536 | tf_op jit(solution)/shard_map/dot_general | solution.py:153
  182.2 0.4 multiply_reduce_fusion.2
  182.6 0.3 multiply_convert_fusion
  182.9 2.3 gather_fusion
  185.3 3.6 %all-to-all-start.1 = ((bf16[8,32,2048]{2,1,0:T(8,128)(2,1)}), bf16[8,32,2048]{2,1,0:T(8,128)(2,1)S(1)}, u32[]{:S(2)}, u32[]{:S(2)}) async-start(bf16[8,32,2048]{2,1,0:T(8,128)(2,1)} %bitcast.20), calls=%async_computation.1 | async-start | bytes 2097152 | tf_op jit(solution)/shard_map/all_to_all | solution.py:174
  188.9 26.5 %all-to-all-done.1 = bf16[8,32,2048]{2,1,0:T(8,128)(2,1)S(1)} async-done(((bf16[8,32,2048]{2,1,0:T(8,128)(2,1)}), bf16[8,32,2048]{2,1,0:T(8,128)(2,1)S(1)}, u32[]{:S(2)}, u32[]{:S(2)}) %all-to-all-start.1) | async-done | bytes 1048608 | tf_op jit(solution)/shard_map/all_to_all | solution.py:174
  215.4 3.1 %fusion.16 = f32[256,512]{1,0:T(8,128)} fusion(bf16[256,2048]{1,0:T(8,128)(2,1)S(1)} %bitcast.141, bf16[1,512,2048]{2,1,0:T(8,128)(2,1)} %all-gather.10.cloned.1.call-done), kind=kOutput, calls=%fused_computation.27 | convolution fusion | flops 536870912 | bytes 3670016 | tf_op jit(solution)/shard_map/emd,ekd->emk/dot_general | solution.py:178
  218.5 3.8 %fusion.12 = bf16[1,256,2048]{2,1,0:T(8,128)(2,1)S(1)} fusion(bf16[1,512,2048]{2,1,0:T(8,128)(2,1)} %all-gather.14.cloned.1.call-done, bf16[256,2048]{1,0:T(8,128)(2,1)S(1)} %bitcast.142, bf16[1,512,2048]{2,1,0:T(8,128)(2,1)} %all-gather.12.cloned.1.call-done, f32[256,512]{1,0:T(8,128)} %fusion.16), kind=kOutput, calls=%fused_computation.23 | convolution fusion | flops 1075052544 | bytes 6815744 | tf_op jit(solution)/shard_map/emk,ekd->emd/dot_general | solution.py:181
  222.4 0.7 fusion.63
  223.0 0.7 fusion.62
  223.7 0.7 fusion.61
  224.3 0.6 fusion.60
  225.0 0.7 fusion.59
  225.7 0.7 fusion.58
  226.3 0.7 fusion.57
  227.0 0.7 fusion.56
  227.7 3.6 %all-to-all-start.2 = ((bf16[8,1,32,2048]{3,2,1,0:T(8,128)(2,1)}), bf16[8,1,32,2048]{3,2,1,0:T(8,128)(2,1)S(1)}, u32[]{:S(2)}, u32[]{:S(2)}) async-start(bf16[8,1,32,2048]{3,2,1,0:T(8,128)(2,1)} %fusion.56), calls=%async_computation.2 | async-start | bytes 2097152 | tf_op jit(solution)/shard_map/all_to_all | solution.py:111
  231.3 26.4 %all-to-all-done.2 = bf16[8,1,32,2048]{3,2,1,0:T(8,128)(2,1)S(1)} async-done(((bf16[8,1,32,2048]{3,2,1,0:T(8,128)(2,1)}), bf16[8,1,32,2048]{3,2,1,0:T(8,128)(2,1)S(1)}, u32[]{:S(2)}, u32[]{:S(2)}) %all-to-all-start.2) | async-done | bytes 1048608 | tf_op jit(solution)/shard_map/all_to_all | solution.py:111
  257.7 2.3 gather_fusion.1
  260.0 2.4 reshape.202
  262.4 3.3 %multiply_reduce_fusion = f32[128,2048]{1,0:T(8,128)S(1)} fusion(f32[128,2,2048]{2,1,0:T(2,128)S(1)} %reshape.202, f32[128,2]{1,0:T(8,128)S(1)} %copy.76), kind=kLoop, calls=%fused_computation.29 | loop fusion | flops 786432 | bytes 3146752 | tf_op jit(solution)/shard_map/reduce_sum | solution.py:185
  265.9 1.2 add_convert_fusion
  (132 shorter events, 5.5 us)
Async XLA Ops:
  6.5 8.9 %copy-start = (bf16[4,64,64]{2,1,0:T(8,128)(2,1)S(1)}, bf16[4,64,64]{2,1,0:T(8,128)(2,1)}, u32[]{:S(2)}) copy-start(bf16[4,64,64]{2,1,0:T(8,128)(2,1)} %param.25) | copy-start | bytes 98308
  6.5 2.3 copy-start.3
  6.5 4.8 %copy-start.10 = (s32[128,2]{0,1:T(2,128)S(1)}, s32[128,2]{0,1:T(2,128)}, u32[]{:S(2)}) copy-start(s32[128,2]{0,1:T(2,128)} %param.33) | copy-start | bytes 3076
  6.5 5.2 %copy-start.9 = (bf16[4,256]{1,0:T(4,128)(2,1)S(1)}, bf16[4,256]{1,0:T(4,128)(2,1)}, u32[]{:S(2)}) copy-start(bf16[4,256]{1,0:T(4,128)(2,1)} %param.24) | copy-start | bytes 6148
  6.5 5.3 %copy-start.12 = (f32[256]{0:T(256)S(1)}, f32[256]{0:T(256)}, u32[]{:S(2)}) copy-start(f32[256]{0:T(256)} %param.27) | copy-start | bytes 3076
  6.5 6.5 %copy-start.8 = (f32[512]{0:T(512)S(1)}, f32[512]{0:T(512)}, u32[]{:S(2)}) copy-start(f32[512]{0:T(512)} %param.28) | copy-start | bytes 6148
  6.6 172.6 %all-gather.8.cloned.1.call-start = ((), (), s32[]{:S(2)}) async-start(), calls=%async_computation.3 | async-start | bytes 5242880 | tf_op jit(solution)/shard_map/all_gather | solution.py:155
  7.3 181.6 %all-gather.10.cloned.1.call-start = ((), (), s32[]{:S(2)}) async-start(), calls=%async_computation.4 | async-start | bytes 2621440 | tf_op jit(solution)/shard_map/all_gather | solution.py:175
  8.0 210.5 %all-gather.12.cloned.1.call-start = ((), (), s32[]{:S(2)}) async-start(), calls=%async_computation.5 | async-start | bytes 2621440 | tf_op jit(solution)/shard_map/all_gather | solution.py:176
  8.8 209.8 %all-gather.14.cloned.1.call-start = ((), (), s32[]{:S(2)}) async-start(), calls=%async_computation.6 | async-start | bytes 2621440 | tf_op jit(solution)/shard_map/all_gather | solution.py:177
  8.9 5.7 %collective-permute-start = (bf16[256,3]{1,0:T(8,128)(2,1)S(1)}, bf16[256,3]{1,0:T(8,128)(2,1)S(1)}, u32[]{:S(2)}, u32[]{:S(2)}) collective-permute-start(bf16[256,3]{1,0:T(8,128)(2,1)S(1)} %slice.49), channel_id=1, source_target_pairs={{0,4},{4,8},{8,12},{12,16},{16,20},{20,24},{24,28},{1,5},{5,9},{9,... | collective-permute-start | bytes 4616 | tf_op jit(solution)/shard_map/ppermute | solution.py:32
  16.4 0.8 copy-start.13
  42.4 126.2 %copy-start.4 = (bf16[256,512]{1,0:T(8,128)(2,1)S(1)}, bf16[256,512]{1,0:T(8,128)(2,1)}, u32[]{:S(2)}) copy-start(bf16[256,512]{1,0:T(8,128)(2,1)} %param.23) | copy-start | bytes 786436
  169.5 9.6 %all-to-all-start = ((bf16[256,4,128]{2,0,1:T(8,128)(2,1)}), bf16[256,4,128]{2,0,1:T(8,128)(2,1)S(1)}, u32[]{:S(2)}, u32[]{:S(2)}) async-start(bf16[256,4,128]{2,0,1:T(8,128)(2,1)} %copy_bitcast_fusion), calls=%async_computation | async-start | bytes 524288 | tf_op jit(solution)/shard_map/all_to_all | solution.py:151
  179.1 3.1 %copy-start.1 = (bf16[128,2048]{1,0:T(8,128)(2,1)S(1)}, bf16[128,2048]{1,0:T(8,128)(2,1)}, u32[]{:S(2)}) copy-start(bf16[128,2048]{1,0:T(8,128)(2,1)} %param.21) | copy-start | bytes 1572868
  179.1 3.1 %copy-start.5 = (f32[2048]{0:T(1024)S(1)}, f32[2048]{0:T(1024)}, u32[]{:S(2)}) copy-start(f32[2048]{0:T(1024)} %param.30) | copy-start | bytes 24580
  179.1 3.5 %copy-start.6 = (f32[2048]{0:T(1024)S(1)}, f32[2048]{0:T(1024)}, u32[]{:S(2)}) copy-start(f32[2048]{0:T(1024)} %param.31) | copy-start | bytes 24580
  185.3 30.1 %all-to-all-start.1 = ((bf16[8,32,2048]{2,1,0:T(8,128)(2,1)}), bf16[8,32,2048]{2,1,0:T(8,128)(2,1)S(1)}, u32[]{:S(2)}, u32[]{:S(2)}) async-start(bf16[8,32,2048]{2,1,0:T(8,128)(2,1)} %bitcast.20), calls=%async_computation.1 | async-start | bytes 2097152 | tf_op jit(solution)/shard_map/all_to_all | solution.py:174
  222.3 8.9 %copy-start.11 = (f32[128,2]{0,1:T(2,128)S(1)}, f32[128,2]{0,1:T(2,128)}, u32[]{:S(2)}) copy-start(f32[128,2]{0,1:T(2,128)} %param.34) | copy-start | bytes 3076
  227.7 30.1 %all-to-all-start.2 = ((bf16[8,1,32,2048]{3,2,1,0:T(8,128)(2,1)}), bf16[8,1,32,2048]{3,2,1,0:T(8,128)(2,1)S(1)}, u32[]{:S(2)}, u32[]{:S(2)}) async-start(bf16[8,1,32,2048]{3,2,1,0:T(8,128)(2,1)} %fusion.56), calls=%async_computation.2 | async-start | bytes 2097152 | tf_op jit(solution)/shard_map/all_to_all | solution.py:111
  262.4 3.5 %copy-start.2 = (bf16[128,2048]{1,0:T(8,128)(2,1)S(1)}, bf16[128,2048]{1,0:T(8,128)(2,1)}, u32[]{:S(2)}) copy-start(bf16[128,2048]{1,0:T(8,128)(2,1)} %param.21) | copy-start | bytes 1572868
  262.4 3.5 %copy-start.7 = (f32[2048]{0:T(1024)S(1)}, f32[2048]{0:T(1024)}, u32[]{:S(2)}) copy-start(f32[2048]{0:T(1024)} %param.32) | copy-start | bytes 24580
Sparse Core Ops, SparseCore 0:
  9.2 55.2 all-gather.7
  66.4 35.1 all-gather.9
  103.4 35.1 all-gather.11
  140.4 35.1 all-gather.13
